TPU v7x, 512 devices: a whole 4x8x8 slice. The times are simulated.
512 devices in a mesh: fs: 64 (over z, y), tp: 8 (over x, core).
Axes of the slice: x: 4, y: 8, z: 8, core: 2. Of those that a mesh axis runs over, the one named last changes fastest.
Arguments:
- tokens: bfloat16 [24576, 2048], P('fs', 'tp'), may hold values from -6 to 6
- outer_gate: bfloat16 [2048, 2048], P('fs', 'tp'), may hold values from -0.125 to 0.125
- inner_gate: bfloat16 [2048, 2048], P('fs', 'tp'), may hold values from -0.125 to 0.125
- mix_value: bfloat16 [2048, 2048], P('fs', 'tp'), may hold values from -0.125 to 0.125
- mix_taps: bfloat16 [3, 2048], P(None, 'tp'), may hold values from -3 to 3
- mix_out: bfloat16 [2048, 2048], P('tp', 'fs'), may hold values from -0.375 to 0.375
- mix_gain: bfloat16 [2048], P('tp'), may hold values from 0.099609375 to 1.8984375
- ffn_gate: bfloat16 [2048, 3072], P('fs', 'tp'), may hold values from -0.125 to 0.125
- ffn_value: bfloat16 [2048, 3072], P('fs', 'tp'), may hold values from -0.125 to 0.125
- gate_taps: bfloat16 [3, 3072], P(None, 'tp'), may hold values from -3 to 3
- value_taps: bfloat16 [3, 3072], P(None, 'tp'), may hold values from -3 to 3
- ffn_down: bfloat16 [3072, 2048], P('tp', 'fs'), may hold values from -0.3125 to 0.3125
- ffn_gain: bfloat16 [2048], P('tp'), may hold values from 0.099609375 to 1.8984375
Outputs:
- layer_out: bfloat16 [24576, 2048], P('fs', 'tp')
All inputs are finite; a program needn't handle non-finite values.
Results may differ from a plain program's by a relative error of at most 0.015.
Values may be sent and summed in bfloat16 or wider, within the bound.
A program may use at most 64 MiB of HBM per device.

v0:
```python
import jax
import jax.numpy as jnp
from jax import lax
from jax.sharding import PartitionSpec as P

SEQ_LEN = 128
residual_scale = 8.0**0.25
norm_epsilon = 1e-05


def copy_for_each(value, axis):
    copies = jnp.broadcast_to(value, (lax.axis_size(axis), *value.shape))
    return lax.all_to_all(copies, axis, split_axis=0, concat_axis=0, tiled=True)


def taken_together(value, axis):
    everything = copy_for_each(value, axis)
    return jnp.sum(everything, axis=0)


def in_one(arrays, axis):
    ends = [0]
    for a in arrays:
        ends.append(ends[-1] + a.size)
    subtotal = taken_together(jnp.concatenate([a.ravel() for a in arrays]), axis)
    return tuple((subtotal[b:e].reshape(a.shape) for a, b, e in zip(arrays, ends, ends[1:])))


def in_one_piece(arrays, axis, dim, along):
    both = jnp.concatenate(arrays, axis=along)
    filled, at, finished = (lax.all_gather(both, axis, axis=dim, tiled=True), 0, [])
    for a in arrays:
        finished.append(lax.slice_in_dim(filled, at, at + a.shape[along], axis=along))
        at += a.shape[along]
    return tuple(finished)


def laid_out(blocks, dim):
    blocks = jnp.moveaxis(blocks, 0, dim)
    dims = blocks.shape
    return blocks.reshape(*dims[:dim], dims[dim] * dims[dim + 1], *dims[dim + 2 :])


def collect(value, axis, dim):
    return laid_out(copy_for_each(value, axis), dim)


def split_up(value, dim, peers):
    before, after = (value.shape[:dim], value.shape[dim + 1 :])
    return jnp.moveaxis(value.reshape(*before, peers, -1, *after), dim, 0)


def sent_and_summed(value, axis, dim):
    peers = lax.axis_size(axis)
    blocks = lax.all_to_all(split_up(value, dim, peers), axis, 0, 0, tiled=True)
    return jnp.sum(blocks.astype(jnp.float32), axis=0)


def stored(values):
    return lax.optimization_barrier(values.astype(jnp.bfloat16)).astype(jnp.float32)


def shift_rows(values, offset):
    position = jnp.arange(values.shape[0]) % SEQ_LEN
    shifted = jnp.concatenate(
        [jnp.zeros((offset, values.shape[1]), values.dtype), values[:-offset]], axis=0
    )
    return jnp.where((position >= offset)[:, None], shifted, jnp.zeros_like(shifted))


def causal_taps(values, taps):
    weights = taps.astype(jnp.float32)
    return (
        values * weights[2]
        + shift_rows(values, 1) * weights[1]
        + shift_rows(values, 2) * weights[0]
    )


def fold_rows(whole, pieces):
    return tuple((jnp.dot(whole, piece, preferred_element_type=jnp.float32) for piece in pieces))


def norm_shares(prenorm, gain):
    width = prenorm.shape[1] * lax.axis_size("tp")
    row_sums = jnp.sum(prenorm, axis=1)
    row_squares = jnp.sum(prenorm * prenorm, axis=1)
    total, total_squares = in_one((row_sums, row_squares), "tp")
    mean = total / width
    spread = total_squares / width - mean * mean
    scaled = (prenorm - mean[:, None]) * lax.rsqrt(spread[:, None] + norm_epsilon)
    return (scaled * gain.astype(jnp.float32)).astype(jnp.bfloat16)


def body(
    tokens,
    outer_gate,
    inner_gate,
    mix_value,
    mix_taps,
    mix_out,
    mix_gain,
    ffn_gate,
    ffn_value,
    gate_taps,
    value_taps,
    ffn_down,
    ffn_gain,
):
    gate_whole, value_whole = in_one_piece((ffn_gate, ffn_value), "fs", 0, 1)
    whole_tokens = collect(tokens, "tp", 1)
    outer, inner, values = fold_rows(
        whole_tokens, in_one_piece((outer_gate, inner_gate, mix_value), "fs", 0, 1)
    )
    outer, inner, values = (stored(outer), stored(inner), stored(values))
    gated = (outer * causal_taps(inner * values, mix_taps)).astype(jnp.bfloat16)
    mixer_terms = jnp.dot(gated, collect(mix_out, "fs", 1), preferred_element_type=jnp.float32)
    mixer_branch = sent_and_summed(mixer_terms.astype(jnp.bfloat16), "tp", 1)
    first_own = norm_shares(residual_scale * tokens.astype(jnp.float32) + mixer_branch, mix_gain)
    first_whole = collect(first_own, "tp", 1)
    gate_up = jnp.dot(first_whole, gate_whole, preferred_element_type=jnp.float32)
    value_up = jnp.dot(first_whole, value_whole, preferred_element_type=jnp.float32)
    gate_up, value_up = (stored(gate_up), stored(value_up))
    hidden = (
        jax.nn.silu(causal_taps(gate_up, gate_taps)) * causal_taps(value_up, value_taps)
    ).astype(jnp.bfloat16)
    ffn_terms = jnp.dot(
        hidden,
        lax.all_gather(ffn_down, "fs", axis=1, tiled=True),
        preferred_element_type=jnp.float32,
    )
    ffn_branch = sent_and_summed(ffn_terms.astype(jnp.bfloat16), "tp", 1)
    return norm_shares(residual_scale * first_own.astype(jnp.float32) + ffn_branch, ffn_gain)


def solution(mesh):
    placed = (
        P("fs", "tp"),
        P("fs", "tp"),
        P("fs", "tp"),
        P("fs", "tp"),
        P(None, "tp"),
        P("tp", "fs"),
        P("tp"),
        P("fs", "tp"),
        P("fs", "tp"),
        P(None, "tp"),
        P(None, "tp"),
        P("tp", "fs"),
        P("tp"),
    )
    return jax.shard_map(body, mesh=mesh, in_specs=placed, out_specs=P("fs", "tp"), check_vma=False)
```

profile of v0, /device:TPU:1, one launch (start us, length us, event | category | flops | bytes accessed | tf_op | source)
XLA Modules:
  0.0 324.7 jit_solution(7652189762097484057)
XLA Ops:
  6.5 1.4 pad_maximum_fusion
  7.9 0.0 all-gather.4.cloned.1.call-update
  7.9 0.0 all-gather.6.cloned.1.call-start
  8.0 1.4 pad_maximum_fusion.1
  9.4 0.0 all-gather.6.cloned.1.call-update
  9.4 1.1 copy.25
  10.5 0.1 broadcast_in_dim.65
  10.6 0.0 copy-start.1
  10.6 29.8 %all_to_all.37 = bf16[8,384,256]{1,2,0:T(8,128)(2,1)S(1)} all-to-all(bf16[8,384,256]{1,2,0:T(8,128)(2,1)S(1)} %broadcast_in_dim.65), channel_id=1, replica_groups=mesh['fs'=64,'tp'=8] {'tp'}, dimensions={0} | all-to-all | bytes 3145728 | tf_op jit(solution)/shard_map/all_to_all | solution.py:13
  40.5 1.1 broadcast_in_dim.68
  41.6 12.7 %all-to-all-start.1 = ((bf16[64,256,32]{1,2,0:T(8,128)(2,1)}), bf16[64,256,32]{1,2,0:T(8,128)(2,1)S(1)}, u32[]{:S(2)}, u32[]{:S(2)}) async-start(bf16[64,256,32]{1,2,0:T(8,128)(2,1)} %broadcast_in_dim.68), calls=%async_computation.1 | async-start | bytes 2097152 | tf_op jit(solution)/shard_map/all_to_all | solution.py:13
  54.3 0.0 copy-done.2
  54.3 53.7 %all-gather.4.cloned.1.call-done = bf16[2048,768]{1,0:T(8,128)(2,1)} async-done(((bf16[32,768]{1,0:T(8,128)(2,1)}), bf16[2048,768]{1,0:T(8,128)(2,1)}) %all-gather.4.cloned.1.call-update) | async-done | bytes 3145744 | tf_op jit(solution)/shard_map/all_gather | solution.py:31
  108.0 2.0 fusion.11
  110.0 2.0 fusion.12
  112.0 2.0 fusion.10
  114.0 0.0 all-to-all-done.1
  114.0 1.0 convolution_convert_fusion.1
  115.1 1.3 copy.42
  116.3 8.6 %all-to-all-start.2 = ((bf16[8,384,256]{2,1,0:T(8,128)(2,1)}), bf16[8,384,256]{2,1,0:T(8,128)(2,1)S(1)}, u32[]{:S(2)}, u32[]{:S(2)}) async-start(bf16[8,384,256]{2,1,0:T(8,128)(2,1)} %bitcast.38), calls=%async_computation.2 | async-start | bytes 3145728 | tf_op jit(solution)/shard_map/all_to_all | solution.py:55
  124.9 0.0 all-gather.8.cloned.1.call-start
  125.0 0.7 all-gather.8.cloned.1.call-update
  125.7 19.8 %all-to-all-done.2 = bf16[8,384,256]{2,1,0:T(8,128)(2,1)S(1)} async-done(((bf16[8,384,256]{2,1,0:T(8,128)(2,1)}), bf16[8,384,256]{2,1,0:T(8,128)(2,1)S(1)}, u32[]{:S(2)}, u32[]{:S(2)}) %all-to-all-start.2) | async-done | bytes 1572896 | tf_op jit(solution)/shard_map/all_to_all | solution.py:55
  145.5 0.2 convert_reduce_fusion.1
  145.7 0.2 fusion.34
  145.9 0.6 broadcast_in_dim.69
  146.6 4.2 %all-to-all-start.3 = ((f32[8,1,768]{2,1,0:T(1,128)}), f32[8,1,768]{2,1,0:T(1,128)S(1)}, u32[]{:S(2)}, u32[]{:S(2)}) async-start(f32[8,1,768]{2,1,0:T(1,128)} %broadcast_in_dim.69), calls=%async_computation.3 | async-start | bytes 49152 | tf_op jit(solution)/shard_map/all_to_all | solution.py:13
  150.8 4.7 %all-to-all-done.3 = f32[8,1,768]{2,1,0:T(1,128)S(1)} async-done(((f32[8,1,768]{2,1,0:T(1,128)}), f32[8,1,768]{2,1,0:T(1,128)S(1)}, u32[]{:S(2)}, u32[]{:S(2)}) %all-to-all-start.3) | async-done | bytes 24608 | tf_op jit(solution)/shard_map/all_to_all | solution.py:13
  155.5 0.2 multiply_convert_fusion.2
  155.7 0.2 copy.28
  155.9 1.3 broadcast_in_dim.70
  157.2 4.3 %all-to-all-start.4 = ((bf16[8,384,256]{1,2,0:T(8,128)(2,1)}), bf16[8,384,256]{1,2,0:T(8,128)(2,1)S(1)}, u32[]{:S(2)}, u32[]{:S(2)}) async-start(bf16[8,384,256]{1,2,0:T(8,128)(2,1)} %broadcast_in_dim.70), calls=%async_computation.4 | async-start | bytes 3145728 | tf_op jit(solution)/shard_map/all_to_all | solution.py:13
  161.5 0.6 slice_reduce_fusion.2
  162.2 30.5 %all-gather.6.cloned.1.call-done = bf16[2048,768]{1,0:T(8,128)(2,1)} async-done(((bf16[32,768]{1,0:T(8,128)(2,1)}), bf16[2048,768]{1,0:T(8,128)(2,1)}) %all-gather.6.cloned.1.call-update) | async-done | bytes 3145744 | tf_op jit(solution)/shard_map/all_gather | solution.py:31
  192.7 0.0 all-to-all-done.4
  192.7 2.6 fusion.4
  195.4 1.0 fusion.7
  196.4 0.0 copy-start.5
  196.5 78.2 %all-gather.8.cloned.1.call-done = bf16[384,2048]{0,1:T(8,128)(2,1)} async-done(((bf16[384,32]{0,1:T(8,128)(2,1)}), bf16[384,2048]{0,1:T(8,128)(2,1)}) %all-gather.8.cloned.1.call-update) | async-done | bytes 1572880 | tf_op jit(solution)/shard_map/all_gather | solution.py:129
  274.7 2.9 convolution_convert_fusion
  277.6 0.1 copy.41
  277.7 29.6 %all_to_all.38 = bf16[8,384,256]{2,1,0:T(8,128)(2,1)S(1)} all-to-all(bf16[8,384,256]{2,1,0:T(8,128)(2,1)S(1)} %bitcast.45), channel_id=1, replica_groups=mesh['fs'=64,'tp'=8] {'tp'}, dimensions={0} | all-to-all | bytes 3145728 | tf_op jit(solution)/shard_map/all_to_all | solution.py:55
  307.3 0.2 convert_reduce_fusion
  307.5 0.2 fusion.35
  307.7 0.6 broadcast_in_dim.73
  308.3 4.3 %all-to-all-start.6 = ((f32[8,1,768]{2,1,0:T(1,128)}), f32[8,1,768]{2,1,0:T(1,128)S(1)}, u32[]{:S(2)}, u32[]{:S(2)}) async-start(f32[8,1,768]{2,1,0:T(1,128)} %broadcast_in_dim.73), calls=%async_computation.6 | async-start | bytes 49152 | tf_op jit(solution)/shard_map/all_to_all | solution.py:13
  312.6 4.7 %all-to-all-done.6 = f32[8,1,768]{2,1,0:T(1,128)S(1)} async-done(((f32[8,1,768]{2,1,0:T(1,128)}), f32[8,1,768]{2,1,0:T(1,128)S(1)}, u32[]{:S(2)}, u32[]{:S(2)}) %all-to-all-start.6) | async-done | bytes 24608 | tf_op jit(solution)/shard_map/all_to_all | solution.py:13
  317.4 0.9 multiply_convert_fusion.1
  (43 shorter events, 0.4 us)
Async XLA Ops:
  6.5 101.5 %all-gather.4.cloned.1.call-start = ((), (), s32[]{:S(2)}) async-start(), calls=%async_computation.7 | async-start | bytes 3194880 | tf_op jit(solution)/shard_map/all_gather | solution.py:31
  7.9 184.7 %all-gather.6.cloned.1.call-start = ((), (), s32[]{:S(2)}) async-start(), calls=%async_computation.8 | async-start | bytes 3194880 | tf_op jit(solution)/shard_map/all_gather | solution.py:31
  10.6 29.8 %copy-start.1 = (bf16[256,32]{0,1:T(8,128)(2,1)S(1)}, bf16[256,32]{0,1:T(8,128)(2,1)}, u32[]{:S(2)}) copy-start(bf16[256,32]{0,1:T(8,128)(2,1)} %param.18) | copy-start | bytes 49156
  40.5 13.8 %copy-start.2 = (bf16[3,256]{1,0:T(4,128)(2,1)S(1)}, bf16[3,256]{1,0:T(4,128)(2,1)}, u32[]{:S(2)}) copy-start(bf16[3,256]{1,0:T(4,128)(2,1)} %param.17) | copy-start | bytes 4612
  41.6 72.4 %all-to-all-start.1 = ((bf16[64,256,32]{1,2,0:T(8,128)(2,1)}), bf16[64,256,32]{1,2,0:T(8,128)(2,1)S(1)}, u32[]{:S(2)}, u32[]{:S(2)}) async-start(bf16[64,256,32]{1,2,0:T(8,128)(2,1)} %broadcast_in_dim.68), calls=%async_computation.1 | async-start | bytes 2097152 | tf_op jit(solution)/shard_map/all_to_all | solution.py:13
  54.3 59.7 %copy-start.7 = (pred[384]{0:T(512)(128)(4,1)}, pred[384]{0:T(512)(128)(4,1)S(1)}, u32[]{:S(2)}) copy-start(pred[384]{0:T(512)(128)(4,1)S(1)} %get-tuple-element.22) | copy-start | bytes 1156
  54.3 59.7 %copy-start.9 = (pred[384]{0:T(512)(128)(4,1)}, pred[384]{0:T(512)(128)(4,1)S(1)}, u32[]{:S(2)}) copy-start(pred[384]{0:T(512)(128)(4,1)S(1)} %get-tuple-element.23) | copy-start | bytes 1156
  116.3 29.2 %all-to-all-start.2 = ((bf16[8,384,256]{2,1,0:T(8,128)(2,1)}), bf16[8,384,256]{2,1,0:T(8,128)(2,1)S(1)}, u32[]{:S(2)}, u32[]{:S(2)}) async-start(bf16[8,384,256]{2,1,0:T(8,128)(2,1)} %bitcast.38), calls=%async_computation.2 | async-start | bytes 3145728 | tf_op jit(solution)/shard_map/all_to_all | solution.py:55
  124.9 20.8 %copy-start = (bf16[384,256]{1,0:T(8,128)(2,1)S(1)}, bf16[384,256]{1,0:T(8,128)(2,1)}, u32[]{:S(2)}) copy-start(bf16[384,256]{1,0:T(8,128)(2,1)} %param.13) | copy-start | bytes 589828
  124.9 25.9 %copy-start.12 = (bf16[256]{0:T(256)(128)(2,1)S(1)}, bf16[256]{0:T(256)(128)(2,1)}, u32[]{:S(2)}) copy-start(bf16[256]{0:T(256)(128)(2,1)} %param.19) | copy-start | bytes 1540
  124.9 149.7 %all-gather.8.cloned.1.call-start = ((), (), s32[]{:S(2)}) async-start(), calls=%async_computation.9 | async-start | bytes 1597440 | tf_op jit(solution)/shard_map/all_gather | solution.py:129
  146.6 8.9 %all-to-all-start.3 = ((f32[8,1,768]{2,1,0:T(1,128)}), f32[8,1,768]{2,1,0:T(1,128)S(1)}, u32[]{:S(2)}, u32[]{:S(2)}) async-start(f32[8,1,768]{2,1,0:T(1,128)} %broadcast_in_dim.69), calls=%async_computation.3 | async-start | bytes 49152 | tf_op jit(solution)/shard_map/all_to_all | solution.py:13
  157.2 4.3 %copy-start.3 = (bf16[3,384]{1,0:T(4,128)(2,1)S(1)}, bf16[3,384]{1,0:T(4,128)(2,1)}, u32[]{:S(2)}) copy-start(bf16[3,384]{1,0:T(4,128)(2,1)} %param.22) | copy-start | bytes 6916
  157.2 4.3 %copy-start.4 = (bf16[3,384]{1,0:T(4,128)(2,1)S(1)}, bf16[3,384]{1,0:T(4,128)(2,1)}, u32[]{:S(2)}) copy-start(bf16[3,384]{1,0:T(4,128)(2,1)} %param.23) | copy-start | bytes 6916
  157.2 35.5 %all-to-all-start.4 = ((bf16[8,384,256]{1,2,0:T(8,128)(2,1)}), bf16[8,384,256]{1,2,0:T(8,128)(2,1)S(1)}, u32[]{:S(2)}, u32[]{:S(2)}) async-start(bf16[8,384,256]{1,2,0:T(8,128)(2,1)} %broadcast_in_dim.70), calls=%async_computation.4 | async-start | bytes 3145728 | tf_op jit(solution)/shard_map/all_to_all | solution.py:13
  192.7 2.7 copy-start.11
  196.4 78.3 %copy-start.5 = (f32[384]{0:T(512)S(1)}, f32[384]{0:T(512)}, u32[]{:S(2)}) copy-start(f32[384]{0:T(512)} %get-tuple-element.25) | copy-start | bytes 4612
  196.4 78.3 %copy-start.6 = (f32[384]{0:T(512)S(1)}, f32[384]{0:T(512)}, u32[]{:S(2)}) copy-start(f32[384]{0:T(512)} %get-tuple-element.26) | copy-start | bytes 4612
  196.4 78.3 %copy-start.8 = (pred[384]{0:T(512)(128)(4,1)S(1)}, pred[384]{0:T(512)(128)(4,1)}, u32[]{:S(2)}) copy-start(pred[384]{0:T(512)(128)(4,1)} %copy-done.7) | copy-start | bytes 1156
  196.4 78.3 %copy-start.10 = (pred[384]{0:T(512)(128)(4,1)S(1)}, pred[384]{0:T(512)(128)(4,1)}, u32[]{:S(2)}) copy-start(pred[384]{0:T(512)(128)(4,1)} %copy-done.9) | copy-start | bytes 1156
  307.3 5.3 %copy-start.13 = (bf16[256]{0:T(256)(128)(2,1)S(1)}, bf16[256]{0:T(256)(128)(2,1)}, u32[]{:S(2)}) copy-start(bf16[256]{0:T(256)(128)(2,1)} %param.25) | copy-start | bytes 1540
  308.3 9.0 %all-to-all-start.6 = ((f32[8,1,768]{2,1,0:T(1,128)}), f32[8,1,768]{2,1,0:T(1,128)S(1)}, u32[]{:S(2)}, u32[]{:S(2)}) async-start(f32[8,1,768]{2,1,0:T(1,128)} %broadcast_in_dim.73), calls=%async_computation.6 | async-start | bytes 49152 | tf_op jit(solution)/shard_map/all_to_all | solution.py:13
Sparse Core Ops, SparseCore 0:
  10.3 97.6 all-gather.3
  111.0 81.5 all-gather.5
  195.7 78.9 all-gather.7
where the time goes:
time: 326 us; the launch traced here: 325 us
  waiting for transfers between devices  192 us (59%)
  blocking collectives  59.4 us (18%)
  starting transfers between devices  34.1 us (10%)
  matrix products  13.4 us (4%)
  between operations  13.4 us (4%)
  local copies, waits for them, and re-layouts  7.32 us (2%)
  other arithmetic  4.73 us (1%)
    all_gather x2, waiting for transfers between devices, in_one_piece(): lax.all_gather(both, axis, axis=dim, tiled=True)  84.2 us
    all_gather x1, waiting for transfers between devices, body(): lax.all_gather(ffn_down, 'fs', axis=1, tiled=True)  78.2 us
    all_to_all x1, blocking collectives, copy_for_each(): return lax.all_to_all(copies, axis, split_axis=0, concat_axis=0, tiled=True)  29.8 us
    all_to_all x1, blocking collectives, sent_and_summed(): blocks = lax.all_to_all(split_up(value, dim, peers), axis, 0, 0, tiled=True)  29.6 us
    all_to_all x4, starting transfers between devices, copy_for_each(): return lax.all_to_all(copies, axis, split_axis=0, concat_axis=0, tiled=True)  25.5 us
    all_to_all x1, waiting for transfers between devices, sent_and_summed(): blocks = lax.all_to_all(split_up(value, dim, peers), axis, 0, 0, tiled=True)  19.8 us
    all_to_all x4, waiting for transfers between devices, copy_for_each(): return lax.all_to_all(copies, axis, split_axis=0, concat_axis=0, tiled=True)  9.4 us
    all_to_all x1, starting transfers between devices, sent_and_summed(): blocks = lax.all_to_all(split_up(value, dim, peers), axis, 0, 0, tiled=True)  8.57 us
  transfers between devices with their start and end apart: 8, of which 6 were waited for; matrix products, arithmetic and copies ran while one was open for 6% of the time, Pallas kernels for 0%

commit v1 on v0

--- a/solution.py
+++ b/solution.py
@@ -6,6 +6,14 @@
 SEQ_LEN = 128
 residual_scale = 8.0**0.25
 norm_epsilon = 1e-05
+
+
+def tiled_gather(array, axis, dim):
+    size = lax.axis_size(axis)
+    repeats = [size if d == dim else 1 for d in range(array.ndim)]
+    return lax.all_to_all(
+        jnp.tile(array, repeats), axis, split_axis=dim, concat_axis=dim, tiled=True
+    )
 
 
 def copy_for_each(value, axis):
@@ -124,11 +132,7 @@
     hidden = (
         jax.nn.silu(causal_taps(gate_up, gate_taps)) * causal_taps(value_up, value_taps)
     ).astype(jnp.bfloat16)
-    ffn_terms = jnp.dot(
-        hidden,
-        lax.all_gather(ffn_down, "fs", axis=1, tiled=True),
-        preferred_element_type=jnp.float32,
-    )
+    ffn_terms = jnp.dot(hidden, tiled_gather(ffn_down, "fs", 1), preferred_element_type=jnp.float32)
     ffn_branch = sent_and_summed(ffn_terms.astype(jnp.bfloat16), "tp", 1)
     return norm_shares(residual_scale * first_own.astype(jnp.float32) + ffn_branch, ffn_gain)
 

time: 326 us -> 281 us (0.86)
  waiting for transfers between devices: 192 us -> 101 us
  blocking collectives: 59.4 us -> 108 us
  starting transfers between devices: 34.1 us -> 29.8 us
    all_gather x1 -> x0, waiting for transfers between devices: 78.2 us -> none  [body(): lax.all_gather(ffn_down, 'fs', axis=1, tiled=True)]
    all_to_all x1 -> x2, blocking collectives: 29.6 us -> 54.1 us  [sent_and_summed(): blocks = lax.all_to_all(split_up(value, dim, peers), axis, 0, 0, tiled=True)]
    all_to_all x1 -> x2, blocking collectives: 29.8 us -> 54.2 us  [copy_for_each(): return lax.all_to_all(copies, axis, split_axis=0, concat_axis=0, tiled=True)]
    all_gather x2, waiting for transfers between devices: 84.2 us -> 60.2 us  [in_one_piece(): lax.all_gather(both, axis, axis=dim, tiled=True)]
    all_to_all x1, waiting for transfers between devices: 19.8 us -> 30.9 us  [tiled_gather(): lax.all_to_all(jnp.tile(array, repeats), axis, split_axis=dim, concat_axi...]
    all_to_all x4 -> x3, starting transfers between devices: 25.5 us -> 21.2 us  [copy_for_each(): return lax.all_to_all(copies, axis, split_axis=0, concat_axis=0, tiled=True)]
    all_to_all x4 -> x3, waiting for transfers between devices: 9.4 us -> 9.45 us  [copy_for_each(): return lax.all_to_all(copies, axis, split_axis=0, concat_axis=0, tiled=True)]
  transfers between devices with their start and end apart: 8 -> 6, of which waited for: 6 -> 5; matrix products, arithmetic and copies ran while one was open for 6% -> 7% of each run, Pallas kernels for 0% -> 0%
where the time goes in v1:
time: 281 us; the launch traced here: 280 us
  blocking collectives  108 us (38%)
  waiting for transfers between devices  101 us (36%)
  starting transfers between devices  29.8 us (11%)
  matrix products  13.7 us (5%)
  between operations  13.7 us (5%)
  local copies, waits for them, and re-layouts  9.85 us (4%)
  other arithmetic  3.98 us (1%)
    all_gather x2, waiting for transfers between devices, in_one_piece(): lax.all_gather(both, axis, axis=dim, tiled=True)  60.2 us
    all_to_all x2, blocking collectives, copy_for_each(): return lax.all_to_all(copies, axis, split_axis=0, concat_axis=0, tiled=True)  54.2 us
    all_to_all x2, blocking collectives, sent_and_summed(): blocks = lax.all_to_all(split_up(value, dim, peers), axis, 0, 0, tiled=True)  54.1 us
    all_to_all x1, waiting for transfers between devices, tiled_gather(): lax.all_to_all(jnp.tile(array, repeats), axis, split_axis=dim, concat_axi...  30.9 us
    all_to_all x3, starting transfers between devices, copy_for_each(): return lax.all_to_all(copies, axis, split_axis=0, concat_axis=0, tiled=True)  21.2 us
    all_to_all x3, waiting for transfers between devices, copy_for_each(): return lax.all_to_all(copies, axis, split_axis=0, concat_axis=0, tiled=True)  9.45 us
    all_to_all x1, starting transfers between devices, tiled_gather(): lax.all_to_all(jnp.tile(array, repeats), axis, split_axis=dim, concat_axi...  8.61 us
    dot_general x3, matrix products, fold_rows(): jnp.dot(whole, piece, preferred_element_type=jnp.float32)  5.89 us
  transfers between devices with their start and end apart: 6, of which 5 were waited for; matrix products, arithmetic and copies ran while one was open for 7% of the time, Pallas kernels for 0%

profile of v1, /device:TPU:1, one launch (start us, length us, event | category | flops | bytes accessed | tf_op | source)
XLA Modules:
  0.0 280.0 jit_solution(8978210921865760302)
XLA Ops:
  6.5 1.4 pad_maximum_fusion
  7.9 0.0 all-gather.3.cloned.1.call-update
  7.9 1.1 copy.26
  9.0 0.1 broadcast_in_dim.65
  9.2 0.0 copy-start.5
  9.2 29.8 %all_to_all.46 = bf16[8,384,256]{1,2,0:T(8,128)(2,1)S(1)} all-to-all(bf16[8,384,256]{1,2,0:T(8,128)(2,1)S(1)} %broadcast_in_dim.65), channel_id=1, replica_groups=mesh['fs'=64,'tp'=8] {'tp'}, dimensions={0} | all-to-all | bytes 3145728 | tf_op jit(solution)/shard_map/all_to_all | solution.py:21
  39.0 1.1 broadcast_in_dim.68
  40.2 12.6 %all-to-all-start.1 = ((bf16[64,256,32]{1,2,0:T(8,128)(2,1)}), bf16[64,256,32]{1,2,0:T(8,128)(2,1)S(1)}, u32[]{:S(2)}, u32[]{:S(2)}) async-start(bf16[64,256,32]{1,2,0:T(8,128)(2,1)} %broadcast_in_dim.68), calls=%async_computation.1 | async-start | bytes 2097152 | tf_op jit(solution)/shard_map/all_to_all | solution.py:21
  52.8 0.0 all-gather.5.cloned.1.call-start
  52.9 0.6 pad_maximum_fusion.1
  53.5 0.1 all-gather.5.cloned.1.call-update
  53.6 57.8 %all-gather.3.cloned.1.call-done = bf16[2048,768]{1,0:T(8,128)(2,1)} async-done(((bf16[32,768]{1,0:T(8,128)(2,1)}), bf16[2048,768]{1,0:T(8,128)(2,1)}) %all-gather.3.cloned.1.call-update) | async-done | bytes 3145744 | tf_op jit(solution)/shard_map/all_gather | solution.py:39
  111.4 2.0 fusion.11
  113.4 2.0 fusion.12
  115.3 2.0 fusion.10
  117.4 1.0 convolution_convert_fusion.1
  118.4 0.1 copy.43
  118.5 28.9 %all_to_all.47 = bf16[8,384,256]{2,1,0:T(8,128)(2,1)S(1)} all-to-all(bf16[8,384,256]{2,1,0:T(8,128)(2,1)S(1)} %bitcast.46), channel_id=1, replica_groups=mesh['fs'=64,'tp'=8] {'tp'}, dimensions={0} | all-to-all | bytes 3145728 | tf_op jit(solution)/shard_map/all_to_all | solution.py:63
  147.5 0.2 convert_reduce_fusion.1
  147.7 0.7 copy-done
  148.4 0.2 fusion.34
  148.6 0.6 broadcast_in_dim.69
  149.2 4.3 %all-to-all-start.3 = ((f32[8,1,768]{2,1,0:T(1,128)}), f32[8,1,768]{2,1,0:T(1,128)S(1)}, u32[]{:S(2)}, u32[]{:S(2)}) async-start(f32[8,1,768]{2,1,0:T(1,128)} %broadcast_in_dim.69), calls=%async_computation.3 | async-start | bytes 49152 | tf_op jit(solution)/shard_map/all_to_all | solution.py:21
  153.5 4.8 %all-to-all-done.3 = f32[8,1,768]{2,1,0:T(1,128)S(1)} async-done(((f32[8,1,768]{2,1,0:T(1,128)}), f32[8,1,768]{2,1,0:T(1,128)S(1)}, u32[]{:S(2)}, u32[]{:S(2)}) %all-to-all-start.3) | async-done | bytes 24608 | tf_op jit(solution)/shard_map/all_to_all | solution.py:21
  158.3 0.2 multiply_convert_fusion.2
  158.5 0.2 copy.29
  158.6 0.1 broadcast_in_dim.70
  158.8 0.0 copy-start.4
  158.8 24.4 %all_to_all.48 = bf16[8,384,256]{1,2,0:T(8,128)(2,1)} all-to-all(bf16[8,384,256]{1,2,0:T(8,128)(2,1)S(1)} %broadcast_in_dim.70), channel_id=1, replica_groups=mesh['fs'=64,'tp'=8] {'tp'}, dimensions={0} | all-to-all | bytes 3145728 | tf_op jit(solution)/shard_map/all_to_all | solution.py:21
  183.2 1.3 tile.2
  184.4 8.6 %all-to-all-start.5 = ((bf16[384,64,32]{0,2,1:T(8,128)(2,1)}), bf16[384,64,32]{0,2,1:T(8,128)(2,1)S(1)}, u32[]{:S(2)}, u32[]{:S(2)}) async-start(bf16[384,64,32]{0,2,1:T(8,128)(2,1)} %tile.2), calls=%async_computation.5 | async-start | bytes 3145728 | tf_op jit(solution)/shard_map/all_to_all | solution.py:14
  193.1 0.6 slice_reduce_fusion.2
  193.7 2.4 all-gather.5.cloned.1.call-done
  196.2 3.0 %fusion.4 = bf16[384,384]{1,0:T(8,128)(2,1)S(1)} fusion(bf16[384,2048]{0,1:T(8,128)(2,1)} %bitcast.52, bf16[2048,768]{1,0:T(8,128)(2,1)} %all-gather.5.cloned.1.call-done), kind=kOutput, calls=%fused_computation.10 | convolution fusion | flops 604127232 | bytes 3440640 | tf_op jit(solution)/shard_map/dot_general | solution.py:129
  199.3 1.3 copy-done.1
  200.6 1.0 fusion.7
  201.6 0.8 slice.112
  202.5 0.8 slice.114
  203.3 30.9 %all-to-all-done.5 = bf16[384,64,32]{0,2,1:T(8,128)(2,1)S(1)} async-done(((bf16[384,64,32]{0,2,1:T(8,128)(2,1)}), bf16[384,64,32]{0,2,1:T(8,128)(2,1)S(1)}, u32[]{:S(2)}, u32[]{:S(2)}) %all-to-all-start.5) | async-done | bytes 1572896 | tf_op jit(solution)/shard_map/all_to_all | solution.py:14
  234.2 2.8 convolution_convert_fusion
  237.0 0.1 copy.42
  237.1 25.2 %all_to_all.49 = bf16[8,384,256]{2,1,0:T(8,128)(2,1)S(1)} all-to-all(bf16[8,384,256]{2,1,0:T(8,128)(2,1)S(1)} %bitcast.47), channel_id=1, replica_groups=mesh['fs'=64,'tp'=8] {'tp'}, dimensions={0} | all-to-all | bytes 3145728 | tf_op jit(solution)/shard_map/all_to_all | solution.py:63
  262.3 0.2 convert_reduce_fusion
  262.5 0.2 fusion.35
  262.7 0.6 broadcast_in_dim.73
  263.3 4.3 %all-to-all-start.7 = ((f32[8,1,768]{2,1,0:T(1,128)}), f32[8,1,768]{2,1,0:T(1,128)S(1)}, u32[]{:S(2)}, u32[]{:S(2)}) async-start(f32[8,1,768]{2,1,0:T(1,128)} %broadcast_in_dim.73), calls=%async_computation.7 | async-start | bytes 49152 | tf_op jit(solution)/shard_map/all_to_all | solution.py:21
  267.6 4.7 %all-to-all-done.7 = f32[8,1,768]{2,1,0:T(1,128)S(1)} async-done(((f32[8,1,768]{2,1,0:T(1,128)}), f32[8,1,768]{2,1,0:T(1,128)S(1)}, u32[]{:S(2)}, u32[]{:S(2)}) %all-to-all-start.7) | async-done | bytes 24608 | tf_op jit(solution)/shard_map/all_to_all | solution.py:21
  272.3 0.9 multiply_convert_fusion.1
  (41 shorter events, 0.3 us)
Async XLA Ops:
  6.5 104.9 %all-gather.3.cloned.1.call-start = ((), (), s32[]{:S(2)}) async-start(), calls=%async_computation.8 | async-start | bytes 3194880 | tf_op jit(solution)/shard_map/all_gather | solution.py:39
  9.2 29.8 %copy-start.5 = (bf16[256,32]{0,1:T(8,128)(2,1)S(1)}, bf16[256,32]{0,1:T(8,128)(2,1)}, u32[]{:S(2)}) copy-start(bf16[256,32]{0,1:T(8,128)(2,1)} %param.18) | copy-start | bytes 49156
  39.0 13.8 %copy-start.2 = (bf16[32,384]{1,0:T(8,128)(2,1)S(1)}, bf16[32,384]{1,0:T(8,128)(2,1)}, u32[]{:S(2)}) copy-start(bf16[32,384]{1,0:T(8,128)(2,1)} %param.21) | copy-start | bytes 73732
  39.0 13.8 %copy-start.3 = (bf16[32,384]{1,0:T(8,128)(2,1)S(1)}, bf16[32,384]{1,0:T(8,128)(2,1)}, u32[]{:S(2)}) copy-start(bf16[32,384]{1,0:T(8,128)(2,1)} %param.20) | copy-start | bytes 73732
  39.0 14.5 %copy-start.6 = (bf16[3,256]{1,0:T(4,128)(2,1)S(1)}, bf16[3,256]{1,0:T(4,128)(2,1)}, u32[]{:S(2)}) copy-start(bf16[3,256]{1,0:T(4,128)(2,1)} %param.17) | copy-start | bytes 4612
  40.2 77.2 %all-to-all-start.1 = ((bf16[64,256,32]{1,2,0:T(8,128)(2,1)}), bf16[64,256,32]{1,2,0:T(8,128)(2,1)S(1)}, u32[]{:S(2)}, u32[]{:S(2)}) async-start(bf16[64,256,32]{1,2,0:T(8,128)(2,1)} %broadcast_in_dim.68), calls=%async_computation.1 | async-start | bytes 2097152 | tf_op jit(solution)/shard_map/all_to_all | solution.py:21
  52.8 143.4 %all-gather.5.cloned.1.call-start = ((), (), s32[]{:S(2)}) async-start(), calls=%async_computation.9 | async-start | bytes 3194880 | tf_op jit(solution)/shard_map/all_gather | solution.py:39
  53.6 63.8 %copy-start.9 = (pred[384]{0:T(512)(128)(4,1)}, pred[384]{0:T(512)(128)(4,1)S(1)}, u32[]{:S(2)}) copy-start(pred[384]{0:T(512)(128)(4,1)S(1)} %get-tuple-element.22) | copy-start | bytes 1156
  53.6 63.8 %copy-start.10 = (pred[384]{0:T(512)(128)(4,1)}, pred[384]{0:T(512)(128)(4,1)S(1)}, u32[]{:S(2)}) copy-start(pred[384]{0:T(512)(128)(4,1)S(1)} %get-tuple-element.23) | copy-start | bytes 1156
  147.4 0.9 copy-start
  147.4 6.0 %copy-start.12 = (bf16[256]{0:T(256)(128)(2,1)S(1)}, bf16[256]{0:T(256)(128)(2,1)}, u32[]{:S(2)}) copy-start(bf16[256]{0:T(256)(128)(2,1)} %param.19) | copy-start | bytes 1540
  149.2 9.0 %all-to-all-start.3 = ((f32[8,1,768]{2,1,0:T(1,128)}), f32[8,1,768]{2,1,0:T(1,128)S(1)}, u32[]{:S(2)}, u32[]{:S(2)}) async-start(f32[8,1,768]{2,1,0:T(1,128)} %broadcast_in_dim.69), calls=%async_computation.3 | async-start | bytes 49152 | tf_op jit(solution)/shard_map/all_to_all | solution.py:21
  158.8 24.4 %copy-start.4 = (bf16[384,32]{0,1:T(8,128)(2,1)S(1)}, bf16[384,32]{0,1:T(8,128)(2,1)}, u32[]{:S(2)}) copy-start(bf16[384,32]{0,1:T(8,128)(2,1)} %param.24) | copy-start | bytes 73732
  184.4 8.6 %copy-start.7 = (bf16[3,384]{1,0:T(4,128)(2,1)S(1)}, bf16[3,384]{1,0:T(4,128)(2,1)}, u32[]{:S(2)}) copy-start(bf16[3,384]{1,0:T(4,128)(2,1)} %param.22) | copy-start | bytes 6916
  184.4 8.6 %copy-start.8 = (bf16[3,384]{1,0:T(4,128)(2,1)S(1)}, bf16[3,384]{1,0:T(4,128)(2,1)}, u32[]{:S(2)}) copy-start(bf16[3,384]{1,0:T(4,128)(2,1)} %param.23) | copy-start | bytes 6916
  184.4 49.8 %all-to-all-start.5 = ((bf16[384,64,32]{0,2,1:T(8,128)(2,1)}), bf16[384,64,32]{0,2,1:T(8,128)(2,1)S(1)}, u32[]{:S(2)}, u32[]{:S(2)}) async-start(bf16[384,64,32]{0,2,1:T(8,128)(2,1)} %tile.2), calls=%async_computation.5 | async-start | bytes 3145728 | tf_op jit(solution)/shard_map/all_to_all | solution.py:14
  196.2 3.1 %copy-start.11 = (bf16[2048,768]{1,0:T(8,128)(2,1)S(1)}, bf16[2048,768]{1,0:T(8,128)(2,1)}, u32[]{:S(2)}) copy-start(bf16[2048,768]{1,0:T(8,128)(2,1)} %all-gather.5.cloned.1.call-done) | copy-start | bytes 9437188
  199.2 1.4 copy-start.1
  262.3 5.3 %copy-start.13 = (bf16[256]{0:T(256)(128)(2,1)S(1)}, bf16[256]{0:T(256)(128)(2,1)}, u32[]{:S(2)}) copy-start(bf16[256]{0:T(256)(128)(2,1)} %param.25) | copy-start | bytes 1540
  263.3 9.0 %all-to-all-start.7 = ((f32[8,1,768]{2,1,0:T(1,128)}), f32[8,1,768]{2,1,0:T(1,128)S(1)}, u32[]{:S(2)}, u32[]{:S(2)}) async-start(f32[8,1,768]{2,1,0:T(1,128)} %broadcast_in_dim.73), calls=%async_computation.7 | async-start | bytes 49152 | tf_op jit(solution)/shard_map/all_to_all | solution.py:21
Sparse Core Ops, SparseCore 0:
  10.3 101.0 all-gather.2
  114.4 81.7 all-gather.4
